TPU v7x, 32 devices: a whole 2x2x4 slice. The times are simulated.
32 devices in a mesh: ep: 4 (over y, x), tp: 8 (over z, core).
Axes of the slice: x: 2, y: 2, z: 4, core: 2. Of those that a mesh axis runs over, the one named last changes fastest.
Arguments:
- tokens: bfloat16 [8192, 2048], P(('ep', 'tp')), may hold values from -6 to 6
- norm_gain: float32 [2048], replicated, may hold values from 0.1 to 1.9
- expert_ids: int32 [8192, 2], P(('ep', 'tp')), may hold values from 0 to 3, all different within a row; in each aligned block of 256 rows (0 to 255, 256 to 511, ...) at most 256 rows name the same one
- gate_weights: float32 [8192, 2], P(('ep', 'tp')), may hold values from 0.2 to 1
- w_gate: bfloat16 [4, 2048, 1024], P('ep', None, 'tp'), may hold values from -0.125 to 0.125
- w_up: bfloat16 [4, 2048, 1024], P('ep', None, 'tp'), may hold values from -0.125 to 0.125
- w_down: bfloat16 [4, 2048, 1024], P('ep', None, 'tp'), may hold values from -0.1875 to 0.1875
- dense_gate: bfloat16 [2048, 256], P('ep'), may hold values from -0.125 to 0.125
- dense_up: bfloat16 [2048, 256], P('ep'), may hold values from -0.125 to 0.125
- dense_down: bfloat16 [256, 2048], P(None, 'ep'), may hold values from -0.375 to 0.375
- mix_vector: float32 [2048], replicated, may hold values from -0.125 to 0.125
Outputs:
- mixed: bfloat16 [8192, 2048], P(('ep', 'tp'))
Inputs may be any that keep to these rules, and one draw needn't show every extreme that they name: `expert_ids`: A row names 2 different experts. In the rows of one device (aligned blocks of 256 rows) each expert is named by at most 256 rows, a bound that some block reaches.
All inputs are finite; a program needn't handle non-finite values.
Results may differ from a plain program's by a relative error of at most 0.0075.
Values may be sent and summed in bfloat16 or wider, within the bound.
A program may use at most 320 MiB of HBM per device.

v0:
```python
import jax
import jax.numpy as jnp
from jax import lax
from jax.sharding import PartitionSpec as P

eps = 1e-06


def dense_branch(normed, dense_gate, dense_up, dense_down, mix_vector):
    dense_g = jnp.dot(
        normed,
        lax.all_gather(dense_gate, "ep", axis=0, tiled=True),
        preferred_element_type=jnp.float32,
    )
    dense_u = jnp.dot(
        normed,
        lax.all_gather(dense_up, "ep", axis=0, tiled=True),
        preferred_element_type=jnp.float32,
    )
    dense_hidden = (jax.nn.silu(dense_g) * dense_u).astype(jnp.bfloat16)
    dense_out = jnp.dot(
        dense_hidden,
        lax.all_gather(dense_down, "ep", axis=1, tiled=True),
        preferred_element_type=jnp.float32,
    )
    mix = jax.nn.sigmoid(jnp.sum(normed.astype(jnp.float32) * mix_vector, axis=1))
    return mix[:, None] * dense_out


def on_device(
    tokens,
    norm_gain,
    expert_ids,
    gate_weights,
    w_gate,
    w_up,
    w_down,
    dense_gate,
    dense_up,
    dense_down,
    mix_vector,
):
    values = tokens.astype(jnp.float32)
    scale = lax.rsqrt(jnp.mean(values * values, axis=1, keepdims=True) + eps)
    normed = (values * scale * norm_gain).astype(jnp.bfloat16)
    count_tok, topk = expert_ids.shape
    width = tokens.shape[1]
    groups = lax.axis_size("ep")
    capacity = 2 * count_tok * topk // groups
    flat_ids = expert_ids.reshape(-1)
    onehot = (flat_ids[:, None] == jnp.arange(groups, dtype=jnp.int32)[None, :]).astype(jnp.int32)
    before = jnp.cumsum(onehot, axis=0) - onehot
    slot = jnp.sum(before * onehot, axis=1)
    dest = flat_ids * capacity + slot
    owner = jnp.arange(count_tok * topk, dtype=jnp.int32) // topk
    buffer = jnp.zeros((groups * capacity, width), jnp.bfloat16).at[dest].set(normed[owner])
    arrived = lax.all_to_all(
        buffer.reshape(groups, capacity, width), "ep", split_axis=0, concat_axis=0, tiled=True
    )
    rows = arrived.reshape(groups * capacity, width)
    gate = jnp.dot(
        rows,
        lax.all_gather(w_gate, "tp", axis=2, tiled=True)[0],
        preferred_element_type=jnp.float32,
    )
    upper = jnp.dot(
        rows, lax.all_gather(w_up, "tp", axis=2, tiled=True)[0], preferred_element_type=jnp.float32
    )
    hidden_all = (jax.nn.silu(gate) * upper).astype(jnp.bfloat16)
    expert_out = lax.dot_general(
        hidden_all,
        lax.all_gather(w_down, "tp", axis=2, tiled=True)[0],
        (((1,), (1,)), ((), ())),
        preferred_element_type=jnp.float32,
    )
    results = expert_out.astype(jnp.bfloat16).reshape(groups, capacity, width)
    returned = lax.all_to_all(results, "ep", split_axis=0, concat_axis=0, tiled=True)
    picked = returned.reshape(groups * capacity, width)[dest].reshape(count_tok, topk, width)
    routed = jnp.einsum("tk,tkd->td", gate_weights, picked.astype(jnp.float32))
    side = dense_branch(normed, dense_gate, dense_up, dense_down, mix_vector)
    return (routed + side).astype(jnp.bfloat16)


def solution(mesh):
    placed = (
        P(("ep", "tp"), None),
        P(),
        P(("ep", "tp"), None),
        P(("ep", "tp"), None),
        P("ep", None, "tp"),
        P("ep", None, "tp"),
        P("ep", None, "tp"),
        P("ep", None),
        P("ep", None),
        P(None, "ep"),
        P(),
    )
    return jax.shard_map(
        on_device, mesh=mesh, in_specs=placed, out_specs=P(("ep", "tp"), None), check_vma=False
    )
```

profile of v0, /device:TPU:1, one launch (start us, length us, event | category | flops | bytes accessed | tf_op | source)
XLA Modules:
  0.0 275.0 jit_solution(9708944648632882612)
XLA Ops:
  6.5 0.0 all-gather.9.cloned.1.call-start
  6.5 0.7 all-gather.9.cloned.1.call-update
  7.3 0.0 all-gather.7.cloned.1.call-start
  7.3 0.7 all-gather.7.cloned.1.call-update
  8.0 0.0 all-gather.11.cloned.1.call-start
  8.1 0.7 all-gather.11.cloned.1.call-update
  8.7 0.8 copy.13
  9.6 0.1 eq.29
  9.7 0.1 eq.25
  9.9 1.2 reduce-window.6
  11.1 0.2 slice_reduce_fusion
  11.3 0.2 reduce-window.9
  11.5 0.7 broadcast_multiply_fusion
  12.2 0.1 copy.12
  12.3 0.1 mul.66
  12.5 0.1 add_bitcast_fusion
  12.6 1.5 fusion.13
  14.1 1.8 multiply_reduce_fusion
  15.9 12.8 %scatter_custom_fusion = bf16[1024,2048]{1,0:T(8,128)(2,1)} fusion(s32[512]{0:T(512)S(1)} %bitcast.54, bf16[256,2048]{1,0:T(8,128)(2,1)S(1)} %get-tuple-element.6, s32[1024]{0:T(1024)S(1)} %pad_clamp_fusion.1, bf16[]{:T(256)} %constant.31.clone.1), kind=kCustom, calls=%fused_computation.19 | custom fusion | bytes 4194306 | tf_op jit(solution)/shard_map/scatter | solution.py:56
  28.7 4.9 %all-to-all-start = ((bf16[4,256,2048]{2,1,0:T(8,128)(2,1)}), bf16[4,256,2048]{2,1,0:T(8,128)(2,1)}, u32[]{:S(2)}, u32[]{:S(2)}) async-start(bf16[4,256,2048]{2,1,0:T(8,128)(2,1)} %bitcast.52), calls=%async_computation | async-start | bytes 8388608 | tf_op jit(solution)/shard_map/all_to_all | solution.py:57
  33.6 0.0 all-gather.13.cloned.1.call-start
  33.7 0.5 all-gather.13.cloned.1.call-update
  34.2 47.1 %all-to-all-done = bf16[4,256,2048]{2,1,0:T(8,128)(2,1)} async-done(((bf16[4,256,2048]{2,1,0:T(8,128)(2,1)}), bf16[4,256,2048]{2,1,0:T(8,128)(2,1)}, u32[]{:S(2)}, u32[]{:S(2)}) %all-to-all-start) | async-done | bytes 4194336 | tf_op jit(solution)/shard_map/all_to_all | solution.py:57
  81.3 0.0 all-gather.9.cloned.1.call-done
  81.3 10.0 %fusion.2 = f32[1024,1024]{1,0:T(8,128)} fusion(bf16[1024,2048]{1,0:T(8,128)(2,1)} %bitcast.5, bf16[1,2048,1024]{2,1,0:T(8,128)(2,1)} %all-gather.9.cloned.1.call-done), kind=kOutput, calls=%fused_computation.5 | convolution fusion | flops 4294967296 | bytes 12582912 | tf_op jit(solution)/shard_map/dot_general | solution.py:66
  91.3 15.6 %all-gather.7.cloned.1.call-done = bf16[1,2048,1024]{2,1,0:T(8,128)(2,1)} async-done(((bf16[1,2048,128]{2,1,0:T(8,128)(2,1)}), bf16[1,2048,1024]{2,1,0:T(8,128)(2,1)}) %all-gather.7.cloned.1.call-update) | async-done | bytes 4194320 | tf_op jit(solution)/shard_map/all_gather | solution.py:63
  106.9 9.5 %multiply_convert_fusion = bf16[1024,1024]{1,0:T(8,128)(2,1)S(1)} fusion(f32[1024,1024]{1,0:T(8,128)} %fusion.2, bf16[1024,2048]{1,0:T(8,128)(2,1)} %bitcast.5, bf16[1,2048,1024]{2,1,0:T(8,128)(2,1)} %all-gather.7.cloned.1.call-done), kind=kOutput, calls=%fused_computation.9 | convolution fusion | flops 4301258752 | bytes 14680064 | tf_op jit(solution)/shard_map/dot_general | solution.py:61
  116.5 38.1 %all-gather.11.cloned.1.call-done = bf16[1,2048,1024]{2,1,0:T(8,128)(2,1)} async-done(((bf16[1,2048,128]{2,1,0:T(8,128)(2,1)}), bf16[1,2048,1024]{2,1,0:T(8,128)(2,1)}) %all-gather.11.cloned.1.call-update) | async-done | bytes 4194320 | tf_op jit(solution)/shard_map/all_gather | solution.py:72
  154.6 8.3 %fusion.6 = bf16[1024,2048]{1,0:T(8,128)(2,1)} fusion(bf16[1024,1024]{1,0:T(8,128)(2,1)S(1)} %multiply_convert_fusion, bf16[1,2048,1024]{2,1,0:T(8,128)(2,1)} %all-gather.11.cloned.1.call-done), kind=kOutput, calls=%fused_computation.10 | convolution fusion | flops 4297064448 | bytes 10485760 | tf_op jit(solution)/shard_map/dot_general | solution.py:70
  162.9 0.0 copy-start
  162.9 5.0 %all-to-all-start.1 = ((bf16[4,256,2048]{2,1,0:T(8,128)(2,1)}), bf16[4,256,2048]{2,1,0:T(8,128)(2,1)}, u32[]{:S(2)}, u32[]{:S(2)}) async-start(bf16[4,256,2048]{2,1,0:T(8,128)(2,1)} %bitcast.53), calls=%async_computation.1 | async-start | bytes 8388608 | tf_op jit(solution)/shard_map/all_to_all | solution.py:77
  167.8 0.0 all-gather.15.cloned.1.call-start
  167.9 0.5 all-gather.15.cloned.1.call-update
  168.4 0.3 all-gather.17.cloned.1.call-start
  168.7 0.3 all-gather.17.cloned.1.call-update
  169.0 0.0 copy-done
  169.0 0.2 copy.15
  169.2 36.4 %all-gather.13.cloned.1.call-done = bf16[2048,256]{1,0:T(8,128)(2,1)} async-done(((bf16[512,256]{1,0:T(8,128)(2,1)}), bf16[2048,256]{1,0:T(8,128)(2,1)}) %all-gather.13.cloned.1.call-update) | async-done | bytes 1048592 | tf_op jit(solution)/shard_map/all_gather | solution.py:12
  205.6 1.7 fusion.33
  207.3 16.2 %all-to-all-done.1 = bf16[4,256,2048]{2,1,0:T(8,128)(2,1)} async-done(((bf16[4,256,2048]{2,1,0:T(8,128)(2,1)}), bf16[4,256,2048]{2,1,0:T(8,128)(2,1)}, u32[]{:S(2)}, u32[]{:S(2)}) %all-to-all-start.1) | async-done | bytes 4194336 | tf_op jit(solution)/shard_map/all_to_all | solution.py:77
  223.5 7.1 %gather_fusion = bf16[512,2048]{1,0:T(8,128)(2,1)S(1)} fusion(bf16[1024,2048]{1,0:T(8,128)(2,1)} %bitcast.10, s32[1024]{0:T(1024)S(1)} %pad_clamp_fusion), kind=kCustom, calls=%fused_computation.1 | custom fusion | bytes 4196352 | tf_op jit(solution)/shard_map/gather | solution.py:78
  230.6 2.6 reshape.125
  233.3 3.9 %fusion.32 = f32[256,1,2048]{2,1,0:T(1,128)S(1)} fusion(bf16[256,2,2048]{2,1,0:T(2,128)(2,1)} %reshape.125, bf16[256,2,1]{1,2,0:T(2,128)(2,1)S(1)} %copy.15), kind=kOutput, calls=%fused_computation.52 | convolution fusion | flops 2097152 | bytes 4195328 | tf_op jit(solution)/shard_map/tk,tkd->td/dot_general | solution.py:79
  237.2 0.0 all-gather.15.cloned.1.call-done
  237.2 26.9 %all-gather.17.cloned.1.call-done = bf16[256,2048]{1,0:T(8,128)(2,1)} async-done(((bf16[256,512]{1,0:T(8,128)(2,1)}), bf16[256,2048]{1,0:T(8,128)(2,1)}) %all-gather.17.cloned.1.call-update) | async-done | bytes 1048592 | tf_op jit(solution)/shard_map/all_gather | solution.py:23
  264.1 4.0 %fusion.12 = bf16[256,2048]{1,0:T(8,128)(2,1)} fusion(bf16[256,2048]{1,0:T(8,128)(2,1)} %all-gather.17.cloned.1.call-done, f32[256,1,2048]{2,1,0:T(1,128)S(1)} %fusion.32, bf16[256,2048]{1,0:T(8,128)(2,1)S(1)} %get-tuple-element.6, bf16[2048,256]{1,0:T(8,128)(2,1)} %all-gather.15.cloned.1.call-done, f32[256]{0:T(256)S(1)} %add_divide_fusion, ...), kind=kOutput, calls=%fused_computation.15 | convolution fusion | flops 538836992 | bytes 6554624 | tf_op jit(solution)/shard_map/dot_general | solution.py:21
  (8 shorter events, 0.1 us)
Async XLA Ops:
  6.5 74.7 %all-gather.9.cloned.1.call-start = ((), (), s32[]{:S(2)}) async-start(), calls=%async_computation.3 | async-start | bytes 4718592 | tf_op jit(solution)/shard_map/all_gather | solution.py:67
  7.3 99.7 %all-gather.7.cloned.1.call-start = ((), (), s32[]{:S(2)}) async-start(), calls=%async_computation.2 | async-start | bytes 4718592 | tf_op jit(solution)/shard_map/all_gather | solution.py:63
  8.0 146.6 %all-gather.11.cloned.1.call-start = ((), (), s32[]{:S(2)}) async-start(), calls=%async_computation.4 | async-start | bytes 4718592 | tf_op jit(solution)/shard_map/all_gather | solution.py:72
  28.7 52.5 %all-to-all-start = ((bf16[4,256,2048]{2,1,0:T(8,128)(2,1)}), bf16[4,256,2048]{2,1,0:T(8,128)(2,1)}, u32[]{:S(2)}, u32[]{:S(2)}) async-start(bf16[4,256,2048]{2,1,0:T(8,128)(2,1)} %bitcast.52), calls=%async_computation | async-start | bytes 8388608 | tf_op jit(solution)/shard_map/all_to_all | solution.py:57
  33.6 172.0 %all-gather.13.cloned.1.call-start = ((), (), s32[]{:S(2)}) async-start(), calls=%async_computation.5 | async-start | bytes 1310720 | tf_op jit(solution)/shard_map/all_gather | solution.py:12
  162.9 6.1 %copy-start = (f32[256,2]{0,1:T(2,128)S(1)}, f32[256,2]{0,1:T(2,128)}, u32[]{:S(2)}) copy-start(f32[256,2]{0,1:T(2,128)} %param.14) | copy-start | bytes 6148
  162.9 60.6 %all-to-all-start.1 = ((bf16[4,256,2048]{2,1,0:T(8,128)(2,1)}), bf16[4,256,2048]{2,1,0:T(8,128)(2,1)}, u32[]{:S(2)}, u32[]{:S(2)}) async-start(bf16[4,256,2048]{2,1,0:T(8,128)(2,1)} %bitcast.53), calls=%async_computation.1 | async-start | bytes 8388608 | tf_op jit(solution)/shard_map/all_to_all | solution.py:77
  167.8 69.4 %all-gather.15.cloned.1.call-start = ((), (), s32[]{:S(2)}) async-start(), calls=%async_computation.6 | async-start | bytes 1310720 | tf_op jit(solution)/shard_map/all_gather | solution.py:17
  168.4 95.7 %all-gather.17.cloned.1.call-start = ((), (), s32[]{:S(2)}) async-start(), calls=%async_computation.7 | async-start | bytes 1310720 | tf_op jit(solution)/shard_map/all_gather | solution.py:23
Sparse Core Ops, SparseCore 0:
  8.9 50.3 all-gather.8
  60.9 45.9 all-gather.6
  108.5 45.9 all-gather.10
  156.3 49.2 all-gather.12
  207.3 28.7 all-gather.14
  237.7 26.3 all-gather.16
where the time goes:
time: 276 us; the launch traced here: 275 us
  waiting for transfers between devices  184 us (67%)
  matrix products  37.4 us (14%)
  local copies, waits for them, and re-layouts  24.3 us (9%)
  between operations  13.6 us (5%)
  starting transfers between devices  10.3 us (4%)
  other arithmetic  5.53 us (2%)
    all_to_all x1, waiting for transfers between devices, on_device(): lax.all_to_all(buffer.reshape(groups, capacity, width), 'ep', split_axis=...  47.1 us
    all_gather x1, waiting for transfers between devices, on_device(): lax.all_gather(w_down, 'tp', axis=2, tiled=True)[0]  38.1 us
    all_gather x1, waiting for transfers between devices, dense_branch(): lax.all_gather(dense_gate, 'ep', axis=0, tiled=True)  36.4 us
    all_gather x1, waiting for transfers between devices, dense_branch(): lax.all_gather(dense_down, 'ep', axis=1, tiled=True)  26.9 us
    all_to_all x1, waiting for transfers between devices, on_device(): lax.all_to_all(results, 'ep', split_axis=0, concat_axis=0, tiled=True)  16.2 us
    all_gather x1, waiting for transfers between devices, on_device(): lax.all_gather(w_gate, 'tp', axis=2, tiled=True)[0]  15.6 us
    scatter x1, local copies, waits for them, and re-layouts, on_device(): jnp.zeros((groups * capacity, width), jnp.bfloat16).at[dest]  12.8 us
    dot_general x1, matrix products, on_device(): jnp.dot(rows, lax.all_gather(w_up, 'tp', axis=2, tiled=True)[0], preferre...  10 us
  transfers between devices with their start and end apart: 8, of which 6 were waited for; matrix products, arithmetic and copies ran while one was open for 23% of the time, Pallas kernels for 0%

commit v1 on v0

--- a/solution.py
+++ b/solution.py
@@ -1,7 +1,337 @@
+import functools
+
 import jax
 import jax.numpy as jnp
 from jax import lax
+from jax.experimental import pallas as pl
+from jax.experimental.pallas import tpu as pltpu
 from jax.sharding import PartitionSpec as P
+
+MESH = pl.DeviceIdType.MESH
+VMEM_BYTES = 65000 * 1024
+CORES = 2
+PIECES = 3
+
+
+def moe_kernel(
+    ne, nz, x_hbm, wg_hbm, wu_hbm, wd_hbm, dg_hbm, du_hbm, dd_hbm, gw_ref, mix_ref, out_ref,
+    xg, ws, dgs, dus, dds, acc, hbuf, ysend, yrecv, side,
+    lsem, wrecv, wright, wleft, wpartner, tsend, trecv, dsend, drecv, rsend, rrecv,
+):
+    me = lax.axis_index("ep")
+    tp = lax.axis_index("tp")
+    z = tp // CORES
+    c = tp % CORES
+    rows, width = xg.shape[1], xg.shape[2]
+    peers = [(me + k) % ne for k in range(1, ne)]
+    partner = z * CORES + (1 - c)
+
+    local = [pltpu.make_async_copy(x_hbm, xg.at[me], lsem.at[0])]
+    for p, ref in enumerate((wg_hbm, wu_hbm, wd_hbm)):
+        local.append(pltpu.make_async_copy(ref, ws.at[z, c, p], lsem.at[1 + p]))
+    for p, (ref, slot) in enumerate(((dg_hbm, dgs), (du_hbm, dus), (dd_hbm, dds))):
+        local.append(pltpu.make_async_copy(ref, slot.at[me], lsem.at[4 + p]))
+    for copy in local:
+        copy.start()
+
+    barrier = pltpu.get_barrier_semaphore()
+    for peer in peers:
+        pl.semaphore_signal(barrier, inc=1, device_id={"ep": peer}, device_id_type=MESH)
+    pl.semaphore_signal(barrier, inc=1, device_id={"tp": partner}, device_id_type=MESH)
+
+    @pl.when(z > 0)
+    def _():
+        pl.semaphore_signal(barrier, inc=1, device_id={"tp": tp - CORES}, device_id_type=MESH)
+
+    @pl.when(z < nz - 1)
+    def _():
+        pl.semaphore_signal(barrier, inc=1, device_id={"tp": tp + CORES}, device_id_type=MESH)
+
+    neighbours = (z + nz - 1) // nz + (2 * nz - 2 - z) // nz
+    pl.semaphore_wait(barrier, ne + neighbours)
+
+    def weight_copy(src, p, target, sems):
+        return pltpu.make_async_remote_copy(
+            src_ref=ws.at[src, c, p], dst_ref=ws.at[src, c, p],
+            send_sem=sems.at[src, p], recv_sem=wrecv.at[src, c, p],
+            device_id={"tp": target}, device_id_type=MESH,
+        )
+
+    def to_right(src, p):
+        return weight_copy(src, p, tp + CORES, wright)
+
+    def to_left(src, p):
+        return weight_copy(src, p, tp - CORES, wleft)
+
+    def to_partner(src, p):
+        return weight_copy(src, p, partner, wpartner)
+
+    def await_piece(src, color, p):
+        pltpu.make_async_remote_copy(
+            src_ref=ws.at[src, color, p], dst_ref=ws.at[src, color, p],
+            send_sem=wpartner.at[src, p], recv_sem=wrecv.at[src, color, p],
+            device_id={"tp": partner}, device_id_type=MESH,
+        ).wait_recv()
+
+    def token_copy(k, block):
+        return pltpu.make_async_remote_copy(
+            src_ref=xg.at[block], dst_ref=xg.at[block],
+            send_sem=tsend.at[k], recv_sem=trecv.at[block],
+            device_id={"ep": peers[k]}, device_id_type=MESH,
+        )
+
+    def dense_copy(k, p, block):
+        slot = (dgs, dus, dds)[p]
+        return pltpu.make_async_remote_copy(
+            src_ref=slot.at[block], dst_ref=slot.at[block],
+            send_sem=dsend.at[k, p], recv_sem=drecv.at[block, p],
+            device_id={"ep": peers[k]}, device_id_type=MESH,
+        )
+
+    for p in range(PIECES):
+        local[1 + p].wait()
+
+        @pl.when(z < nz - 1)
+        def _():
+            to_right(z, p).start()
+
+        @pl.when(z > 0)
+        def _():
+            to_left(z, p).start()
+
+        to_partner(z, p).start()
+    local[0].wait()
+    for k in range(ne - 1):
+        token_copy(k, me).start()
+
+    def forward(d, p):
+        @pl.when(z >= d)
+        def _():
+            await_piece(z - d, c, p)
+
+            @pl.when(z < nz - 1)
+            def _():
+                to_right(z - d, p).start()
+
+            to_partner(z - d, p).start()
+
+        @pl.when(z + d < nz)
+        def _():
+            await_piece(z + d, c, p)
+
+            @pl.when(z > 0)
+            def _():
+                to_left(z + d, p).start()
+
+            to_partner(z + d, p).start()
+
+    def hidden(src):
+        await_piece(src, 1 - c, 0)
+        await_piece(src, 1 - c, 1)
+
+        def one(b, carry):
+            x = xg[b]
+            wg = jnp.concatenate([ws[src, i, 0] for i in range(CORES)], axis=1)
+            g = jnp.dot(x, wg, preferred_element_type=jnp.float32)
+            wu = jnp.concatenate([ws[src, i, 1] for i in range(CORES)], axis=1)
+            u = jnp.dot(x, wu, preferred_element_type=jnp.float32)
+            hbuf[src, b] = (g / (1.0 + jnp.exp(-g)) * u).astype(jnp.bfloat16)
+            return carry
+
+        lax.fori_loop(0, ne, one, 0)
+
+    step = 512
+
+    def down(src, first):
+        await_piece(src, 1 - c, 2)
+
+        def one(b, carry):
+            h = hbuf[src, b]
+            for j in range(0, width, step):
+                w = jnp.concatenate([ws[src, i, 2, j : j + step, :] for i in range(CORES)], axis=1)
+                y = lax.dot_general(
+                    h, w, (((1,), (1,)), ((), ())), preferred_element_type=jnp.float32
+                )
+                if first:
+                    acc[b, :, j : j + step] = y
+                else:
+                    acc[b, :, j : j + step] += y
+            return carry
+
+        lax.fori_loop(0, ne, one, 0)
+
+    def both(d, fn):
+        @pl.when(z >= d)
+        def _():
+            fn(z - d)
+
+        @pl.when(z + d < nz)
+        def _():
+            fn(z + d)
+
+    if nz > 1:
+        for p in range(PIECES):
+            forward(1, p)
+    for p in range(3):
+        local[4 + p].wait()
+    for k in range(ne - 1):
+        block = peers[k]
+        token_copy(k, block).wait_recv()
+    for p in range(PIECES):
+        for k in range(ne - 1):
+            dense_copy(k, p, me).start()
+    hidden(z)
+    down(z, True)
+    for d in range(2, nz):
+        forward(d, 0)
+        both(d - 1, hidden)
+        forward(d, 1)
+        both(d - 1, lambda src: down(src, False))
+        if d == nz - 1:
+            both(d, hidden)
+        forward(d, 2)
+        if d == 2:
+            dense_side(ne, me, peers, dense_copy, xg, dgs, dus, dds, mix_ref, side)
+    if nz == 2:
+        both(1, hidden)
+    if nz > 1:
+        both(nz - 1, lambda src: down(src, False))
+
+    def back_copy(b, k):
+        return pltpu.make_async_remote_copy(
+            src_ref=ysend.at[b], dst_ref=yrecv.at[me],
+            send_sem=rsend.at[k], recv_sem=rrecv.at[me],
+            device_id={"ep": b}, device_id_type=MESH,
+        )
+
+    def back_wait(s):
+        pltpu.make_async_remote_copy(
+            src_ref=ysend.at[s], dst_ref=yrecv.at[s],
+            send_sem=rsend.at[0], recv_sem=rrecv.at[s],
+            device_id={"ep": s}, device_id_type=MESH,
+        ).wait_recv()
+
+    for k in range(ne):
+        b = (2 * ne - 1 - me + k) % ne
+
+        @pl.when(b != me)
+        def _():
+            ysend[b] = acc[b].astype(jnp.bfloat16)
+            back_copy(b, k).start()
+
+    yrecv[me] = acc[me].astype(jnp.bfloat16)
+
+    for k in range(ne - 1):
+        token_copy(k, me).wait_send()
+        for p in range(PIECES):
+            dense_copy(k, p, me).wait_send()
+
+    for src in range(nz):
+        for p in range(PIECES):
+            @pl.when((z < nz - 1) & (z >= src))
+            def _():
+                to_right(src, p).wait_send()
+
+            @pl.when((z > 0) & (z <= src))
+            def _():
+                to_left(src, p).wait_send()
+
+            to_partner(src, p).wait_send()
+
+    for k in range(ne):
+        b = (2 * ne - 1 - me + k) % ne
+
+        @pl.when(b != me)
+        def _():
+            back_copy(b, k).wait_send()
+            back_wait(b)
+
+    tile = 32
+
+    def combine(i, carry):
+        at = pl.ds(pl.multiple_of(i * tile, tile), tile)
+        weights = gw_ref[at, :]
+        total = side[at, :]
+        for s in range(ne):
+            total = total + weights[:, s : s + 1] * yrecv[s, at, :].astype(jnp.float32)
+        out_ref[at, :] = total.astype(jnp.bfloat16)
+        return carry
+
+    lax.fori_loop(0, rows // tile, combine, 0)
+
+
+def dense_side(ne, me, peers, dense_copy, xg, dgs, dus, dds, mix_ref, side):
+    for k in range(ne - 1):
+        for p in range(PIECES):
+            dense_copy(k, p, peers[k]).wait_recv()
+    deep, wide = dgs.shape[1], dds.shape[2]
+    g = u = None
+    for e in range(ne):
+        x = xg[me, :, e * deep : (e + 1) * deep]
+        ge = jnp.dot(x, dgs[e], preferred_element_type=jnp.float32)
+        ue = jnp.dot(x, dus[e], preferred_element_type=jnp.float32)
+        g, u = (ge, ue) if e == 0 else (g + ge, u + ue)
+    h = (g / (1.0 + jnp.exp(-g)) * u).astype(jnp.bfloat16)
+    for e in range(ne):
+        o = jnp.dot(h, dds[e], preferred_element_type=jnp.float32)
+        side[:, e * wide : (e + 1) * wide] = mix_ref[...] * o
+
+
+def fused_layer(ne, tp, normed, gw, mix, w_gate, w_up, w_down, dense_gate, dense_up, dense_down):
+    nz = tp // CORES
+    rows, width = normed.shape
+    shard = w_gate.shape[2]
+    bf, f32 = jnp.bfloat16, jnp.float32
+    dma = pltpu.SemaphoreType.DMA
+    hbm = pl.BlockSpec(memory_space=pl.ANY)
+    vmem = pl.BlockSpec(memory_space=pltpu.VMEM)
+    flops = 6 * ne * rows * width * shard * tp
+    return pl.pallas_call(
+        functools.partial(moe_kernel, ne, nz),
+        out_shape=jax.ShapeDtypeStruct((rows, width), bf),
+        in_specs=[hbm] * 7 + [vmem] * 2,
+        out_specs=vmem,
+        scratch_shapes=[
+            pltpu.VMEM((ne, rows, width), bf),
+            pltpu.VMEM((nz, CORES, PIECES, width, shard), bf),
+            pltpu.VMEM((ne,) + dense_gate.shape, bf),
+            pltpu.VMEM((ne,) + dense_up.shape, bf),
+            pltpu.VMEM((ne,) + dense_down.shape, bf),
+            pltpu.VMEM((ne, rows, width), f32),
+            pltpu.VMEM((nz, ne, rows, CORES * shard), bf),
+            pltpu.VMEM((ne, rows, width), bf),
+            pltpu.VMEM((ne, rows, width), bf),
+            pltpu.VMEM((rows, width), f32),
+            dma((7,)),
+            dma((nz, CORES, PIECES)),
+            dma((nz, PIECES)),
+            dma((nz, PIECES)),
+            dma((nz, PIECES)),
+            dma((ne,)),
+            dma((ne,)),
+            dma((ne, PIECES)),
+            dma((ne, PIECES)),
+            dma((ne,)),
+            dma((ne,)),
+        ],
+        compiler_params=pltpu.CompilerParams(
+            collective_id=0, has_side_effects=True, vmem_limit_bytes=VMEM_BYTES
+        ),
+        cost_estimate=pl.CostEstimate(
+            flops=flops, bytes_accessed=8 * rows * width, transcendentals=ne * rows * shard * tp
+        ),
+    )(normed, w_gate[0], w_up[0], w_down[0], dense_gate, dense_up, dense_down, gw, mix)
+
+
+def fits(ne, tp, tokens, w_gate, dense_gate):
+    rows, width = tokens.shape
+    shard = w_gate.shape[2]
+    block = rows * width
+    size = 2 * ne * block * 5 + 8 * block + 2 * PIECES * width * shard * tp
+    size += 2 * ne * rows * shard * tp + 6 * ne * dense_gate.size
+    aligned = shard % 128 == 0 and width % 512 == 0 and rows % 32 == 0
+    return tp % CORES == 0 and tp > CORES and aligned and size < VMEM_BYTES * 15 // 16
+
 
 eps = 1e-06
 
@@ -46,6 +376,16 @@
     count_tok, topk = expert_ids.shape
     width = tokens.shape[1]
     groups = lax.axis_size("ep")
+    ring = lax.axis_size("tp")
+    if fits(groups, ring, tokens, w_gate, dense_gate):
+        named = expert_ids[:, :, None] == jnp.arange(groups, dtype=jnp.int32)[None, None, :]
+        gw = jnp.sum(jnp.where(named, gate_weights[:, :, None], 0.0), axis=1)
+        mix = jax.nn.sigmoid(
+            jnp.sum(normed.astype(jnp.float32) * mix_vector, axis=1, keepdims=True)
+        )
+        return fused_layer(
+            groups, ring, normed, gw, mix, w_gate, w_up, w_down, dense_gate, dense_up, dense_down
+        )
     capacity = 2 * count_tok * topk // groups
     flat_ids = expert_ids.reshape(-1)
     onehot = (flat_ids[:, None] == jnp.arange(groups, dtype=jnp.int32)[None, :]).astype(jnp.int32)

time: 276 us -> 168 us (0.61)
  waiting for transfers between devices: 184 us -> 0 us
  Pallas kernels: 0 us -> 160 us
  matrix products: 37.4 us -> 0 us
  local copies, waits for them, and re-layouts: 24.3 us -> 3.92 us
  between operations: 13.6 us -> 0.02 us
  starting transfers between devices: 10.3 us -> 0 us
    pallas_call x0 -> x1, Pallas kernels: none -> 160 us  [fused_layer(): pl.pallas_call(functools.partial(moe_kernel, ne, nz), out_shape=jax.Shape...]
    all_gather x6 -> x0, waiting for transfers between devices: 117 us -> none  [the longest x1 38.1 us: on_device(): lax.all_gather(w_down, 'tp', axis=2, tiled=True)[0]]
    all_to_all x2 -> x0, waiting for transfers between devices: 63.3 us -> none  [the longest x1 47.1 us: on_device(): lax.all_to_all(buffer.reshape(groups, capacity, width), 'ep', split_axis=...]
    dot_general x6 -> x0, matrix products: 37.4 us -> none  [the longest x1 10 us: on_device(): jnp.dot(rows, lax.all_gather(w_up, 'tp', axis=2, tiled=True)[0], preferre...]
    scatter x1 -> x0, local copies, waits for them, and re-layouts: 12.8 us -> none  [on_device(): jnp.zeros((groups * capacity, width), jnp.bfloat16).at[dest]]
    all_to_all x2 -> x0, starting transfers between devices: 9.87 us -> none  [the longest x1 4.96 us: on_device(): lax.all_to_all(results, 'ep', split_axis=0, concat_axis=0, tiled=True)]
    gather x1 -> x0, local copies, waits for them, and re-layouts: 7.13 us -> none  [on_device(): returned.reshape(groups * capacity, width)[dest]]
    unnamed x6 -> x0, waiting for transfers between devices: 3.44 us -> none
  transfers between devices with their start and end apart: 8 -> 0, of which waited for: 6 -> 0; matrix products, arithmetic and copies ran while one was open for 23% -> 0% of each run, Pallas kernels for 0% -> 0%
where the time goes in v1:
time: 168 us
  Pallas kernels  160 us (95%)
  local copies, waits for them, and re-layouts  3.92 us (2%)
  other arithmetic  3.75 us (2%)
    pallas_call x1, Pallas kernels, fused_layer(): pl.pallas_call(functools.partial(moe_kernel, ne, nz), out_shape=jax.Shape...  160 us

profile of v1, /device:TPU:1, one launch (start us, length us, event | category | flops | bytes accessed | tf_op | source)
XLA Modules:
  0.0 168.0 jit_solution(3551736471083895030)
XLA Ops:
  0.0 0.0 copy-start
  0.0 0.0 copy-start.1
  0.0 0.0 copy-start.2
  0.0 1.6 fusion
  1.6 0.7 select_reduce_fusion
  2.3 0.8 copy.17.gw_ref
  3.1 0.0 copy-done
  3.1 0.0 copy-done.1
  3.1 0.0 copy-done.2
  3.1 1.4 multiply_reduce_fusion
  4.6 0.8 copy.18.mix_ref
  5.4 160.3 %shard_map.109 = bf16[256,2048]{1,0:T(8,128)(2,1)} custom-call(bf16[256,2048]{1,0:T(8,128)(2,1)} %get-tuple-element.6.x_hbm, bf16[2048,128]{1,0:T(8,128)(2,1)} %bitcast.5, bf16[2048,128]{1,0:T(8,128)(2,1)} %bitcast.6, bf16[2048,128]{1,0:T(8,128)(2,1)} %bitcast.7, bf16[512,256]{1,0:T(8,128)(2,1)} %dg_hbm.1, bf16[512,256]{1,0:T(8,128)(2,1)} %du_hbm.1, ...), custom_call_target="tpu_custom_call" | custom-call | flops 12884901888 | bytes 4194304 | tf_op jit(solution)/shard_map/pallas_call | solution.py:289
  165.7 2.3 %copy.20 = bf16[256,2048]{1,0:T(8,128)(2,1)} copy(bf16[256,2048]{1,0:T(8,128)(2,1)} %shard_map.109) | data formatting | bytes 2097152
  (2 shorter events, 0.0 us)
Async XLA Ops:
  0.0 3.1 %copy-start = (bf16[256,2048]{1,0:T(8,128)(2,1)S(1)}, bf16[256,2048]{1,0:T(8,128)(2,1)}, u32[]{:S(2)}) copy-start(bf16[256,2048]{1,0:T(8,128)(2,1)} %param.11) | copy-start | bytes 3145732
  0.0 3.1 %copy-start.1 = (f32[2048]{0:T(1024)S(1)}, f32[2048]{0:T(1024)}, u32[]{:S(2)}) copy-start(f32[2048]{0:T(1024)} %param.21) | copy-start | bytes 24580
  0.0 3.1 %copy-start.2 = (f32[2048]{0:T(1024)S(1)}, f32[2048]{0:T(1024)}, u32[]{:S(2)}) copy-start(f32[2048]{0:T(1024)} %param.12) | copy-start | bytes 24580

commit v2 on v1

--- a/solution.py
+++ b/solution.py
@@ -11,12 +11,15 @@
 VMEM_BYTES = 65000 * 1024
 CORES = 2
 PIECES = 3
+LANES = 128
+eps = 1e-06
 
 
 def moe_kernel(
-    ne, nz, x_hbm, wg_hbm, wu_hbm, wd_hbm, dg_hbm, du_hbm, dd_hbm, gw_ref, mix_ref, out_ref,
-    xg, ws, dgs, dus, dds, acc, hbuf, ysend, yrecv, side,
-    lsem, wrecv, wright, wleft, wpartner, tsend, trecv, dsend, drecv, rsend, rrecv,
+    ne, nz, x_hbm, wg_hbm, wu_hbm, wd_hbm, dg_hbm, du_hbm, dd_hbm, ids_hbm, gates_hbm,
+    gain_ref, mixv_ref, out_ref,
+    xg, ws, dgs, dus, dds, acc, hbuf, ysend, yrecv, relay, side, ids, gates, mix_ref, stage, wts,
+    lsem, wrecv, wright, wleft, wpartner, tsend, trecv, gsend, grecv, dsend, drecv, rsend, rrecv,
 ):
     me = lax.axis_index("ep")
     tp = lax.axis_index("tp")
@@ -26,11 +29,13 @@
     peers = [(me + k) % ne for k in range(1, ne)]
     partner = z * CORES + (1 - c)
 
-    local = [pltpu.make_async_copy(x_hbm, xg.at[me], lsem.at[0])]
+    local = [pltpu.make_async_copy(x_hbm, ysend.at[1], lsem.at[0])]
     for p, ref in enumerate((wg_hbm, wu_hbm, wd_hbm)):
         local.append(pltpu.make_async_copy(ref, ws.at[z, c, p], lsem.at[1 + p]))
     for p, (ref, slot) in enumerate(((dg_hbm, dgs), (du_hbm, dus), (dd_hbm, dds))):
         local.append(pltpu.make_async_copy(ref, slot.at[me], lsem.at[4 + p]))
+    local.append(pltpu.make_async_copy(ids_hbm, ids, lsem.at[7]))
+    local.append(pltpu.make_async_copy(gates_hbm, gates, lsem.at[8]))
     for copy in local:
         copy.start()
 
@@ -77,6 +82,13 @@
         return pltpu.make_async_remote_copy(
             src_ref=xg.at[block], dst_ref=xg.at[block],
             send_sem=tsend.at[k], recv_sem=trecv.at[block],
+            device_id={"ep": peers[k]}, device_id_type=MESH,
+        )
+
+    def gate_copy(k, block):
+        return pltpu.make_async_remote_copy(
+            src_ref=wts.at[block], dst_ref=wts.at[block],
+            send_sem=gsend.at[k], recv_sem=grecv.at[block],
             device_id={"ep": peers[k]}, device_id_type=MESH,
         )
 
@@ -100,9 +112,39 @@
             to_left(z, p).start()
 
         to_partner(z, p).start()
-    local[0].wait()
+    for i in (0, 7, 8):
+        local[i].wait()
+    tile = 32
+    lane = lax.broadcasted_iota(jnp.int32, (tile, LANES), 1)
+
+    def norm(i, carry):
+        at = pl.ds(pl.multiple_of(i * tile, tile), tile)
+        named, gate = ids[at, :], gates[at, :]
+        weight = jnp.zeros((tile, LANES), jnp.float32)
+        for k in range(named.shape[1]):
+            weight += jnp.where(named[:, k : k + 1] == lane, gate[:, k : k + 1], 0.0)
+        stage[at, :] = weight
+        v = ysend[1, at, :].astype(jnp.float32)
+        scale = lax.rsqrt(jnp.sum(v * v, axis=1, keepdims=True) * (1.0 / width) + eps)
+        n = (v * scale * gain_ref[...]).astype(jnp.bfloat16)
+        ysend[0, at, :] = n
+        m = jnp.sum(n.astype(jnp.float32) * mixv_ref[...], axis=1, keepdims=True)
+        mix_ref[at, :] = 1.0 / (1.0 + jnp.exp(-m))
+        return carry
+
+    lax.fori_loop(0, rows // tile, norm, 0)
+    staged = [
+        pltpu.make_async_copy(ysend.at[0], xg.at[me], lsem.at[9]),
+        pltpu.make_async_copy(stage, wts.at[me], lsem.at[10]),
+    ]
+    for copy in staged:
+        copy.start()
+    for copy in staged:
+        copy.wait()
     for k in range(ne - 1):
         token_copy(k, me).start()
+    for k in range(ne - 1):
+        gate_copy(k, me).start()
 
     def forward(d, p):
         @pl.when(z >= d)
@@ -142,20 +184,23 @@
 
     step = 512
 
+    def down_block(src, b, first):
+        h = hbuf[src, b]
+        for j in range(0, width, step):
+            w = jnp.concatenate([ws[src, i, 2, j : j + step, :] for i in range(CORES)], axis=1)
+            y = lax.dot_general(
+                h, w, (((1,), (1,)), ((), ())), preferred_element_type=jnp.float32
+            )
+            if first:
+                acc[b, :, j : j + step] = y
+            else:
+                acc[b, :, j : j + step] += y
+
     def down(src, first):
         await_piece(src, 1 - c, 2)
 
         def one(b, carry):
-            h = hbuf[src, b]
-            for j in range(0, width, step):
-                w = jnp.concatenate([ws[src, i, 2, j : j + step, :] for i in range(CORES)], axis=1)
-                y = lax.dot_general(
-                    h, w, (((1,), (1,)), ((), ())), preferred_element_type=jnp.float32
-                )
-                if first:
-                    acc[b, :, j : j + step] = y
-                else:
-                    acc[b, :, j : j + step] += y
+            down_block(src, b, first)
             return carry
 
         lax.fori_loop(0, ne, one, 0)
@@ -169,14 +214,14 @@
         def _():
             fn(z + d)
 
-    if nz > 1:
-        for p in range(PIECES):
-            forward(1, p)
+    for p in range(PIECES):
+        forward(1, p)
     for p in range(3):
         local[4 + p].wait()
     for k in range(ne - 1):
-        block = peers[k]
-        token_copy(k, block).wait_recv()
+        token_copy(k, peers[k]).wait_recv()
+    for k in range(ne - 1):
+        gate_copy(k, peers[k]).wait_recv()
     for p in range(PIECES):
         for k in range(ne - 1):
             dense_copy(k, p, me).start()
@@ -192,37 +237,58 @@
         forward(d, 2)
         if d == 2:
             dense_side(ne, me, peers, dense_copy, xg, dgs, dus, dds, mix_ref, side)
-    if nz == 2:
-        both(1, hidden)
-    if nz > 1:
-        both(nz - 1, lambda src: down(src, False))
-
-    def back_copy(b, k):
+    across, along, diagonal = me + 1 - 2 * (me % 2), (me + 2) % ne, ne - 1 - me
+    half = rows // 2
+
+    def back(k):
+        block = (diagonal, diagonal, across, along, along, across)[k]
+        peer = (across, along, across, along, along, across)[k]
+        low = (0, half, 0, half, 0, half)[k]
+        lands = relay.at[k] if k < 2 else yrecv.at[k % 2 if k < 4 else 1 - k % 2, low : low + half]
         return pltpu.make_async_remote_copy(
-            src_ref=ysend.at[b], dst_ref=yrecv.at[me],
-            send_sem=rsend.at[k], recv_sem=rrecv.at[me],
-            device_id={"ep": b}, device_id_type=MESH,
+            src_ref=ysend.at[block, low : low + half], dst_ref=lands,
+            send_sem=rsend.at[k], recv_sem=rrecv.at[k],
+            device_id={"ep": peer}, device_id_type=MESH,
         )
 
-    def back_wait(s):
-        pltpu.make_async_remote_copy(
-            src_ref=ysend.at[s], dst_ref=yrecv.at[s],
-            send_sem=rsend.at[0], recv_sem=rrecv.at[s],
-            device_id={"ep": s}, device_id_type=MESH,
-        ).wait_recv()
-
-    for k in range(ne):
-        b = (2 * ne - 1 - me + k) % ne
-
-        @pl.when(b != me)
-        def _():
-            ysend[b] = acc[b].astype(jnp.bfloat16)
-            back_copy(b, k).start()
-
-    yrecv[me] = acc[me].astype(jnp.bfloat16)
+    def column(block, at):
+        return jnp.sum(jnp.where(lane == me, wts[block, at, :], 0.0), axis=1, keepdims=True)
+
+    def fill(block, low, relayed):
+        def one(i, carry):
+            at = pl.ds(pl.multiple_of(low + i * tile, tile), tile)
+            v = acc[block, at, :] * column(block, at)
+            if relayed is not None:
+                here = pl.ds(pl.multiple_of(i * tile, tile), tile)
+                v += relay[relayed, here, :].astype(jnp.float32)
+            ysend[block, at, :] = v.astype(jnp.bfloat16)
+            return carry
+
+        lax.fori_loop(0, half // tile, one, 0)
+
+    both(nz - 1, lambda src: await_piece(src, 1 - c, 2))
+    both(nz - 1, lambda src: down_block(src, diagonal, False))
+    fill(diagonal, 0, None)
+    back(0).start()
+    fill(diagonal, half, None)
+    back(1).start()
+    both(nz - 1, lambda src: down_block(src, across, False))
+    fill(across, 0, None)
+    back(2).start()
+    both(nz - 1, lambda src: down_block(src, along, False))
+    fill(along, half, None)
+    back(3).start()
+    both(nz - 1, lambda src: down_block(src, me, False))
+    back(0).wait_recv()
+    fill(along, 0, 0)
+    back(4).start()
+    back(1).wait_recv()
+    fill(across, half, 1)
+    back(5).start()
 
     for k in range(ne - 1):
         token_copy(k, me).wait_send()
+        gate_copy(k, me).wait_send()
         for p in range(PIECES):
             dense_copy(k, p, me).wait_send()
 
@@ -238,22 +304,16 @@
 
             to_partner(src, p).wait_send()
 
-    for k in range(ne):
-        b = (2 * ne - 1 - me + k) % ne
-
-        @pl.when(b != me)
-        def _():
-            back_copy(b, k).wait_send()
-            back_wait(b)
-
-    tile = 32
+    for k in range(6):
+        back(k).wait_send()
+    for k in range(2, 6):
+        back(k).wait_recv()
 
     def combine(i, carry):
         at = pl.ds(pl.multiple_of(i * tile, tile), tile)
-        weights = gw_ref[at, :]
-        total = side[at, :]
-        for s in range(ne):
-            total = total + weights[:, s : s + 1] * yrecv[s, at, :].astype(jnp.float32)
+        total = side[at, :] + acc[me, at, :] * column(me, at)
+        for k in range(2):
+            total = total + yrecv[k, at, :].astype(jnp.float32)
         out_ref[at, :] = total.astype(jnp.bfloat16)
         return carry
 
@@ -277,9 +337,13 @@
         side[:, e * wide : (e + 1) * wide] = mix_ref[...] * o
 
 
-def fused_layer(ne, tp, normed, gw, mix, w_gate, w_up, w_down, dense_gate, dense_up, dense_down):
+def fused_layer(
+    ne, tp, tokens, norm_gain, expert_ids, gate_weights,
+    w_gate, w_up, w_down, dense_gate, dense_up, dense_down, mix_vector,
+):
     nz = tp // CORES
-    rows, width = normed.shape
+    rows, width = tokens.shape
+    topk = expert_ids.shape[1]
     shard = w_gate.shape[2]
     bf, f32 = jnp.bfloat16, jnp.float32
     dma = pltpu.SemaphoreType.DMA
@@ -289,7 +353,7 @@
     return pl.pallas_call(
         functools.partial(moe_kernel, ne, nz),
         out_shape=jax.ShapeDtypeStruct((rows, width), bf),
-        in_specs=[hbm] * 7 + [vmem] * 2,
+        in_specs=[hbm] * 9 + [vmem] * 2,
         out_specs=vmem,
         scratch_shapes=[
             pltpu.VMEM((ne, rows, width), bf),
@@ -300,19 +364,27 @@
             pltpu.VMEM((ne, rows, width), f32),
             pltpu.VMEM((nz, ne, rows, CORES * shard), bf),
             pltpu.VMEM((ne, rows, width), bf),
-            pltpu.VMEM((ne, rows, width), bf),
+            pltpu.VMEM((2, rows, width), bf),
+            pltpu.VMEM((2, rows // 2, width), bf),
             pltpu.VMEM((rows, width), f32),
-            dma((7,)),
+            pltpu.VMEM((rows, topk), jnp.int32),
+            pltpu.VMEM((rows, topk), f32),
+            pltpu.VMEM((rows, 1), f32),
+            pltpu.VMEM((rows, LANES), f32),
+            pltpu.VMEM((ne, rows, LANES), f32),
+            dma((11,)),
             dma((nz, CORES, PIECES)),
             dma((nz, PIECES)),
             dma((nz, PIECES)),
             dma((nz, PIECES)),
             dma((ne,)),
             dma((ne,)),
+            dma((ne,)),
+            dma((ne,)),
             dma((ne, PIECES)),
             dma((ne, PIECES)),
-            dma((ne,)),
-            dma((ne,)),
+            dma((6,)),
+            dma((6,)),
         ],
         compiler_params=pltpu.CompilerParams(
             collective_id=0, has_side_effects=True, vmem_limit_bytes=VMEM_BYTES
@@ -320,7 +392,10 @@
         cost_estimate=pl.CostEstimate(
             flops=flops, bytes_accessed=8 * rows * width, transcendentals=ne * rows * shard * tp
         ),
-    )(normed, w_gate[0], w_up[0], w_down[0], dense_gate, dense_up, dense_down, gw, mix)
+    )(
+        tokens, w_gate[0], w_up[0], w_down[0], dense_gate, dense_up, dense_down,
+        expert_ids, gate_weights, norm_gain.reshape(1, width), mix_vector.reshape(1, width),
+    )
 
 
 def fits(ne, tp, tokens, w_gate, dense_gate):
@@ -329,11 +404,8 @@
     block = rows * width
     size = 2 * ne * block * 5 + 8 * block + 2 * PIECES * width * shard * tp
     size += 2 * ne * rows * shard * tp + 6 * ne * dense_gate.size
-    aligned = shard % 128 == 0 and width % 512 == 0 and rows % 32 == 0
-    return tp % CORES == 0 and tp > CORES and aligned and size < VMEM_BYTES * 15 // 16
-
-
-eps = 1e-06
+    aligned = shard % 128 == 0 and width % 512 == 0 and rows % 64 == 0
+    return ne == 4 and tp % CORES == 0 and tp > 2 * CORES and aligned and size < VMEM_BYTES * 15 // 16
 
 
 def dense_branch(normed, dense_gate, dense_up, dense_down, mix_vector):
@@ -370,22 +442,18 @@
     dense_down,
     mix_vector,
 ):
+    groups = lax.axis_size("ep")
+    ring = lax.axis_size("tp")
+    if fits(groups, ring, tokens, w_gate, dense_gate):
+        return fused_layer(
+            groups, ring, tokens, norm_gain, expert_ids, gate_weights,
+            w_gate, w_up, w_down, dense_gate, dense_up, dense_down, mix_vector,
+        )
     values = tokens.astype(jnp.float32)
     scale = lax.rsqrt(jnp.mean(values * values, axis=1, keepdims=True) + eps)
     normed = (values * scale * norm_gain).astype(jnp.bfloat16)
     count_tok, topk = expert_ids.shape
     width = tokens.shape[1]
-    groups = lax.axis_size("ep")
-    ring = lax.axis_size("tp")
-    if fits(groups, ring, tokens, w_gate, dense_gate):
-        named = expert_ids[:, :, None] == jnp.arange(groups, dtype=jnp.int32)[None, None, :]
-        gw = jnp.sum(jnp.where(named, gate_weights[:, :, None], 0.0), axis=1)
-        mix = jax.nn.sigmoid(
-            jnp.sum(normed.astype(jnp.float32) * mix_vector, axis=1, keepdims=True)
-        )
-        return fused_layer(
-            groups, ring, normed, gw, mix, w_gate, w_up, w_down, dense_gate, dense_up, dense_down
-        )
     capacity = 2 * count_tok * topk // groups
     flat_ids = expert_ids.reshape(-1)
     onehot = (flat_ids[:, None] == jnp.arange(groups, dtype=jnp.int32)[None, :]).astype(jnp.int32)

time: 168 us -> 153 us (0.911)
  Pallas kernels: 160 us -> 148 us
  other arithmetic: 3.75 us -> 0 us
    pallas_call x1, Pallas kernels: 160 us -> 148 us  [fused_layer(): pl.pallas_call(functools.partial(moe_kernel, ne, nz), out_shape=jax.Shape...]
    reduce_sum x3 -> x0, other arithmetic: 3.73 us -> none  [the longest x1 1.6 us: on_device(): scale = lax.rsqrt(jnp.mean(values * values, axis=1, keepdims=True) + eps)]
    unnamed x7, local copies, waits for them, and re-layouts: 2.32 us -> 4.58 us
where the time goes in v2:
time: 153 us; the launch traced here: 152 us
  Pallas kernels  148 us (97%)
  local copies, waits for them, and re-layouts  4.58 us (3%)
    pallas_call x1, Pallas kernels, fused_layer(): pl.pallas_call(functools.partial(moe_kernel, ne, nz), out_shape=jax.Shape...  148 us
    unnamed x7, local copies, waits for them, and re-layouts  4.58 us

profile of v2, /device:TPU:1, one launch (start us, length us, event | category | flops | bytes accessed | tf_op | source)
XLA Modules:
  0.0 152.5 jit_solution(301374735613548810)
XLA Ops:
  0.0 0.0 copy-start
  0.0 0.7 copy-done
  0.7 0.0 copy-start.1
  0.7 0.8 copy.12.ids_hbm
  1.5 0.0 copy-done.1
  1.5 0.8 copy.13.gates_hbm
  2.3 147.9 %shard_map.109 = bf16[256,2048]{1,0:T(8,128)(2,1)} custom-call(bf16[256,2048]{1,0:T(8,128)(2,1)} %x_hbm.1, bf16[2048,128]{1,0:T(8,128)(2,1)} %bitcast.5, bf16[2048,128]{1,0:T(8,128)(2,1)} %bitcast.6, bf16[2048,128]{1,0:T(8,128)(2,1)} %bitcast.7, bf16[512,256]{1,0:T(8,128)(2,1)} %dg_hbm.1, bf16[512,256]{1,0:T(8,128)(2,1)} %du_hbm.1, bf16[256,512]{1,0:T(8,128)(2,1)} %dd_hbm.1, ...), custom_call_target="tpu_custom_call" | custom-call | flops 12884901888 | bytes 4194304 | tf_op jit(solution)/shard_map/pallas_call | solution.py:353
  150.2 2.3 %copy.15 = bf16[256,2048]{1,0:T(8,128)(2,1)} copy(bf16[256,2048]{1,0:T(8,128)(2,1)} %shard_map.109) | data formatting | bytes 2097152
Async XLA Ops:
  0.0 0.7 copy-start
  0.7 0.8 copy-start.1
